TPU v7x, 512 devices: a whole 4x4x16 slice. The times are simulated.
512 devices in a mesh: ep: 128 (over z, x, core), tp: 4 (over y).
Axes of the slice: x: 4, y: 4, z: 16, core: 2. Of those that a mesh axis runs over, the one named last changes fastest.
Arguments:
- tokens: bfloat16 [1024, 1024], P('ep'), may hold values from -6 to 6
- kv_cache: bfloat16 [1024, 4, 1024, 128], P('ep', 'tp'), may hold values from -6 to 6
- lengths: int32 [1024], P('ep'), may hold values from 256 to 1024
- w_query: bfloat16 [1024, 512], P(None, 'tp'), may hold values from -0.1875 to 0.1875
- w_key: bfloat16 [1024, 256], P(None, 'tp'), may hold values from -0.1875 to 0.1875
- w_value: bfloat16 [1024, 256], P(None, 'tp'), may hold values from -0.1875 to 0.1875
- break_bias: float32 [8], P('tp'), may hold values from -7.5 to -3.5
- head_gain: float32 [512], P('tp'), may hold values from 0.1 to 1.9
- w_output: bfloat16 [512, 1024], P('tp'), may hold values from -0.25 to 0.25
- attn_norm_gain: float32 [1024], replicated, may hold values from 0.1 to 1.9
- w_router: bfloat16 [1024, 16], replicated, may hold values from -0.1875 to 0.1875
- routes: int32 [1024, 2], P('ep'), may hold values from 0 to 15, all different within a row; in each aligned block of 8 rows (0 to 7, 8 to 15, ...) at most 2 rows name the same one
- expert_gate: bfloat16 [1024, 57344], P(None, ('ep', 'tp')), may hold values from -0.1875 to 0.1875
- expert_up: bfloat16 [1024, 57344], P(None, ('ep', 'tp')), may hold values from -0.1875 to 0.1875
- expert_down: bfloat16 [57344, 1024], P(('ep', 'tp')), may hold values from -0.09375 to 0.09375
- dense_gate: bfloat16 [1024, 2816], P(None, 'ep'), may hold values from -0.1875 to 0.1875
- dense_up: bfloat16 [1024, 2816], P(None, 'ep'), may hold values from -0.1875 to 0.1875
- dense_down: bfloat16 [2816, 1024], P('ep', 'tp'), may hold values from -0.109375 to 0.109375
- mix_gate: bfloat16 [1024], replicated, may hold values from -0.1875 to 0.1875
- ffn_norm_gain: float32 [1024], P('tp'), may hold values from 0.1 to 1.9
Outputs:
- layer_out: bfloat16 [1024, 1024], P('ep', 'tp')
- new_kv: bfloat16 [1024, 4, 128], P('ep', 'tp')
Inputs may be any that keep to these rules, and one draw needn't show every extreme that they name: lengths[b] is the number of valid cached positions of sequence b and the new token's position. `routes`: each row names 2 different experts. Among the rows of one index of ep (aligned blocks of 8 rows) no expert is named more than 2 times, a bound that some block reaches.
All inputs are finite; a program needn't handle non-finite values.
Results may differ from a plain program's by a relative error of at most 0.012.
Values may be sent and summed in bfloat16 or wider, within the bound.
A program may use at most 128 MiB of HBM per device.

v0:
```python
import jax
import jax.numpy as jnp
from jax import lax
from jax.sharding import Mesh
from jax.sharding import PartitionSpec as P

FE = 3584
CAP = 2
EP = ("ep_0", "ep_1", "ep_2")
EP_TP = ("ep_0", "ep_1", "ep_2", "tp")
RESIDUAL_SCALE = 8.0**0.25
PRECISE = lax.Precision.HIGHEST


def from_everyone(shard, axis):
    copies = jnp.broadcast_to(shard, (lax.axis_size(axis), *shard.shape))
    return lax.all_to_all(copies, axis, split_axis=0, concat_axis=0, tiled=True)


def of_everyone(shard, axis):
    everything = from_everyone(shard, axis)
    return jnp.sum(everything.astype(jnp.float32), axis=0)


def cut_along(shard, dim, peers):
    shape = shard.shape
    tiles = shard.reshape(*shape[:dim], peers, shape[dim] // peers, *shape[dim + 1 :])
    return jnp.moveaxis(tiles, dim, 0)


def summed_on_arrival(shard, axis, dim):
    peers = lax.axis_size(axis)
    tiles = lax.all_to_all(cut_along(shard, dim, peers), axis, 0, 0, tiled=True)
    return jnp.sum(tiles.astype(jnp.float32), axis=0)


def joined_along(tiles, dim):
    tiles = jnp.moveaxis(tiles, 0, dim)
    shape = tiles.shape
    return tiles.reshape(*shape[:dim], shape[dim] * shape[dim + 1], *shape[dim + 2 :])


def stacked_from(shard, axes, sequence):
    tiles = shard[None]
    for k in sequence:
        tiles = lax.all_gather(tiles, axes[k], axis=0, tiled=True)
    block = [lax.axis_size(axes[k]) for k in reversed(sequence)]
    tiles = tiles.reshape(*block, *shard.shape)
    turned = sorted(range(len(sequence)), key=lambda place: sequence[len(sequence) - 1 - place])
    return tiles.transpose(*turned, *range(len(sequence), tiles.ndim)).reshape(-1, *shard.shape)


def gathered_by_axis(shard, axes, sequence, dim):
    return joined_along(stacked_from(shard, axes, sequence), dim)


def of_everyone_2(shard, axis):
    return from_everyone(shard, axis).sum(axis=0)


def together(arrays, axis):
    ends = [0]
    for a in arrays:
        ends.append(ends[-1] + a.size)
    so_far = of_everyone_2(jnp.concatenate([a.ravel() for a in arrays]), axis)
    return tuple((so_far[b:e].reshape(a.shape) for a, b, e in zip(arrays, ends, ends[1:])))


def layer_norm(values, gain):
    centre = jnp.mean(values, axis=-1, keepdims=True)
    centred = values - centre
    spread = jnp.mean(centred * centred, axis=-1, keepdims=True)
    return centred * lax.rsqrt(spread + 1e-05) * gain


def stick_weights(scores, visible):
    survive = jnp.where(visible, jax.nn.log_sigmoid(-scores), 0.0)
    remaining = lax.cumsum(survive, axis=3, reverse=True) - survive
    return jnp.where(visible, jnp.exp(jax.nn.log_sigmoid(scores) + remaining), 0.0)


def body(
    tokens,
    kv_cache,
    lengths,
    w_query,
    w_key,
    w_value,
    break_bias,
    head_gain,
    w_output,
    attn_norm_gain,
    w_router,
    routes,
    expert_gate,
    expert_up,
    expert_down,
    dense_gate,
    dense_up,
    dense_down,
    mix_gate,
    ffn_norm_gain,
):
    seq_count = tokens.shape[0]
    model_width = tokens.shape[1]
    key_heads = kv_cache.shape[1]
    positions = kv_cache.shape[2]
    head_dim = kv_cache.shape[3] // 2
    local_heads = w_query.shape[1] // head_dim
    group_size = local_heads // key_heads
    queries = jnp.dot(tokens, w_query, preferred_element_type=jnp.float32).astype(jnp.bfloat16)
    queries = queries.reshape(seq_count, key_heads, group_size, head_dim)
    key_new = jnp.dot(tokens, w_key, preferred_element_type=jnp.float32).astype(jnp.bfloat16)
    value_new = jnp.dot(tokens, w_value, preferred_element_type=jnp.float32).astype(jnp.bfloat16)
    new_kv = jnp.concatenate(
        [
            key_new.reshape(seq_count, key_heads, head_dim),
            value_new.reshape(seq_count, key_heads, head_dim),
        ],
        axis=2,
    )
    cached_keys = kv_cache[..., :head_dim]
    cached_values = kv_cache[..., head_dim:]
    scores = jnp.einsum(
        "bgqd,bgld->bgql", queries, cached_keys, preferred_element_type=jnp.float32
    ) * head_dim ** (-0.5)
    scores = scores + break_bias.reshape(1, key_heads, group_size, 1)
    visible = lax.broadcasted_iota(jnp.int32, (seq_count, 1, 1, positions), 3) < lengths.reshape(
        seq_count, 1, 1, 1
    )
    weights = stick_weights(scores, visible).astype(jnp.bfloat16)
    blended = jnp.einsum(
        "bgql,bgld->bgqd", weights, cached_values, preferred_element_type=jnp.float32
    )
    rescale = lax.rsqrt(jnp.mean(blended * blended, axis=3, keepdims=True) + 1e-06)
    normed = ((blended * rescale).reshape(seq_count, local_heads * head_dim) * head_gain).astype(
        jnp.bfloat16
    )
    partial_out = jnp.dot(normed, w_output, preferred_element_type=jnp.float32)
    attended = of_everyone(partial_out.astype(jnp.bfloat16), "tp").astype(jnp.float32)
    settled = layer_norm(
        RESIDUAL_SCALE * tokens.astype(jnp.float32) + attended, attn_norm_gain
    ).astype(jnp.bfloat16)
    experts = w_router.shape[1]
    top_count = routes.shape[1]
    logits = jnp.dot(settled, w_router, preferred_element_type=jnp.float32)
    chosen = routes[:, :, None] == lax.broadcasted_iota(
        jnp.int32, (seq_count, top_count, experts), 2
    )
    picked = jnp.sum(jnp.where(chosen, logits[:, None, :], 0.0), axis=2)
    route_weight = jax.nn.sigmoid(picked - picked[:, ::-1])
    assigned = chosen.reshape(seq_count * top_count, experts).astype(jnp.int32)
    before = jnp.cumsum(assigned, axis=0) - assigned
    slot_index = jnp.sum(before * assigned, axis=1)
    slot_hits = (
        slot_index[:, None] == lax.broadcasted_iota(jnp.int32, (seq_count * top_count, CAP), 1)
    ).astype(jnp.int32)
    placement = (assigned[:, :, None] * slot_hits[:, None, :]).reshape(
        seq_count, top_count, experts * CAP
    )
    selector = jnp.sum(placement, axis=1).astype(jnp.bfloat16)
    weighted = jnp.sum(placement.astype(jnp.float32) * route_weight[:, :, None], axis=1)
    buffer = lax.dot_general(
        selector, settled, (((0,), (0,)), ((), ())), preferred_element_type=jnp.float32
    )
    buffer = buffer.astype(jnp.bfloat16).reshape(experts, CAP, model_width)
    hosts = lax.axis_size(EP)
    tp_size = lax.axis_size("tp")
    per_host = 1
    outgoing = jnp.repeat(buffer, hosts // experts, axis=0).reshape(hosts, 1, CAP, model_width)
    columns = expert_gate.shape[1]
    block_index = lax.axis_index(EP_TP)
    own_expert = block_index * columns // FE
    local_slot = own_expert - lax.axis_index(EP) * experts // hosts
    slice_width = model_width // tp_size
    arrived = lax.all_to_all(outgoing, EP, split_axis=0, concat_axis=0, tiled=True)
    slot_count = arrived.shape[2]
    received = lax.dynamic_index_in_dim(arrived, local_slot, 1, keepdims=False)
    received = received.reshape(hosts * slot_count, model_width)
    gate_pre = jnp.dot(received, expert_gate, preferred_element_type=jnp.float32)
    up_pre = jnp.dot(received, expert_up, preferred_element_type=jnp.float32)
    hidden = (jax.nn.silu(gate_pre) * up_pre).astype(jnp.bfloat16)
    partial_value = jnp.dot(hidden, expert_down, preferred_element_type=jnp.float32)
    partial_value = partial_value.reshape(hosts, 1, slot_count, model_width)
    slot_mask = (lax.broadcasted_iota(jnp.int32, (1, per_host, 1, 1), 1) == local_slot).astype(
        jnp.float32
    )
    summed = summed_on_arrival((partial_value * slot_mask).astype(jnp.bfloat16), "tp", 3)
    returned = lax.all_to_all(
        summed.astype(jnp.bfloat16), EP, split_axis=0, concat_axis=0, tiled=True
    ).astype(summed.dtype)
    host_ids = lax.broadcasted_iota(jnp.int32, (hosts * per_host,), 0)
    host_expert = host_ids // per_host * experts // hosts + host_ids % per_host
    ownership = (
        host_expert[None, :] == lax.broadcasted_iota(jnp.int32, (experts, hosts * per_host), 0)
    ).astype(jnp.float32)
    gathered = jnp.dot(
        ownership, returned.reshape(hosts * per_host, CAP * slice_width), precision=PRECISE
    )
    gathered = gathered.reshape(experts * CAP, slice_width)
    routed = jnp.dot(weighted, gathered, precision=PRECISE)
    column_rank = lax.axis_index("tp")
    own_settled = lax.dynamic_slice_in_dim(settled, column_rank * slice_width, slice_width, 1)
    shard_rows = lax.all_gather(settled, EP, axis=0, tiled=True)
    gate_pre = jnp.dot(shard_rows, dense_gate, preferred_element_type=jnp.float32)
    up_pre = jnp.dot(shard_rows, dense_up, preferred_element_type=jnp.float32)
    dense_hidden = (jax.nn.silu(gate_pre) * up_pre).astype(jnp.bfloat16)
    own_hidden = lax.all_to_all(dense_hidden, EP, split_axis=0, concat_axis=1, tiled=True)
    dense_out = jnp.dot(
        own_hidden,
        gathered_by_axis(dense_down, EP, (0, 1, 2), 0),
        preferred_element_type=jnp.float32,
    )
    mix_weight = jax.nn.sigmoid(jnp.dot(settled, mix_gate, preferred_element_type=jnp.float32))
    combined = (
        RESIDUAL_SCALE * own_settled.astype(jnp.float32) + routed + mix_weight[:, None] * dense_out
    )
    row_sums, squares = together(
        (jnp.sum(combined, axis=1), jnp.sum(combined * combined, axis=1)), "tp"
    )
    row_mean = row_sums / model_width
    row_var = squares / model_width - row_mean * row_mean
    result = (
        (combined - row_mean[:, None]) * lax.rsqrt(row_var[:, None] + 1e-05) * ffn_norm_gain
    ).astype(jnp.bfloat16)
    return (result, new_kv)


def solution(mesh):
    split = Mesh(mesh.devices.reshape(16, 4, 2, mesh.shape["tp"]), ("ep_0", "ep_1", "ep_2", "tp"))
    return jax.shard_map(
        body,
        mesh=split,
        in_specs=(
            P(EP, None),
            P(EP, "tp", None, None),
            P(EP),
            P(None, "tp"),
            P(None, "tp"),
            P(None, "tp"),
            P("tp"),
            P("tp"),
            P("tp", None),
            P(),
            P(),
            P(EP, None),
            P(None, EP_TP),
            P(None, EP_TP),
            P(EP_TP, None),
            P(None, EP),
            P(None, EP),
            P(EP, "tp"),
            P(),
            P("tp"),
        ),
        out_specs=(P(EP, "tp"), P(EP, "tp", None)),
        check_vma=False,
    )
```

profile of v0, /device:TPU:32, one launch (start us, length us, event | category | flops | bytes accessed | tf_op | source)
XLA Modules:
  0.0 307.2 jit_solution(8504936146442683302)
XLA Ops:
  7.2 0.9 iota_compare_fusion
  8.1 1.1 convolution_convert_fusion.4
  9.3 2.3 fusion.31
  11.6 19.8 %reduce-window.6 = f32[8,1,2,8,128]{4,3,2,1,0:T(8,128)S(1)} reduce-window(f32[8,1,2,8,128]{4,3,2,1,0:T(8,128)S(1)} %bitcast.88, f32[]{:T(128)} %constant.108.clone.1), window={size=1x1x1x1x128 pad=0_0x0_0x0_0x0_0x0_127}, to_apply=%region_0.1 | reduce-window | flops 2080768 | bytes 131076 | tf_op jit(solution)/shard_map/reduce-window
  32.2 1.1 multiply_reduce_fusion.3
  33.7 0.6 broadcast_in_dim.35
  34.3 4.5 %all-to-all-start = ((bf16[4,8,1024]{2,1,0:T(8,128)(2,1)}), bf16[4,8,1024]{2,1,0:T(8,128)(2,1)S(1)}, u32[]{:S(2)}, u32[]{:S(2)}) async-start(bf16[4,8,1024]{2,1,0:T(8,128)(2,1)} %broadcast_in_dim.35), calls=%async_computation | async-start | bytes 131072 | tf_op jit(solution)/shard_map/all_to_all | solution.py:17
  38.8 34.4 %all-gather.1 = bf16[16,22,256]{2,1,0:T(8,128)(2,1)S(1)} all-gather(bf16[1,22,256]{2,1,0:T(8,128)(2,1)S(1)} %bitcast.90), channel_id=2, replica_groups=mesh['ep_0'=16,'ep_1'=4,'ep_2'=2,'tp'=4] {'ep_0'}, dimensions={0}, use_global_device_ids=true | all-gather | bytes 191488 | tf_op jit(solution)/shard_map/all_gather | solution.py:46
  73.2 14.4 %all_gather.14 = bf16[64,22,256]{2,0,1:T(8,128)(2,1)} all-gather(bf16[16,22,256]{2,0,1:T(8,128)(2,1)S(1)} %copy.73), channel_id=1, replica_groups=mesh['ep_0'=16,'ep_1'=4,'ep_2'=2,'tp'=4] {'ep_1'}, dimensions={0}, use_global_device_ids=true | all-gather | bytes 901120 | tf_op jit(solution)/shard_map/all_gather | solution.py:46
  88.6 0.7 multiply_convert_fusion
  89.6 1.0 convolution_convert_fusion
  90.6 1.1 broadcast_in_dim.58
  91.7 12.0 %all-to-all-start.1 = ((bf16[128,1,2,1024]{3,2,1,0:T(2,128)(2,1)}), bf16[128,1,2,1024]{3,2,1,0:T(2,128)(2,1)S(1)}, u32[]{:S(2)}, u32[]{:S(2)}) async-start(bf16[128,1,2,1024]{3,2,1,0:T(2,128)(2,1)} %bitcast.5), calls=%async_computation.1 | async-start | bytes 1048576 | tf_op jit(solution)/shard_map/all_to_all | solution.py:176
  104.0 32.8 %all-to-all-done.1 = bf16[128,1,2,1024]{3,2,1,0:T(2,128)(2,1)S(1)} async-done(((bf16[128,1,2,1024]{3,2,1,0:T(2,128)(2,1)}), bf16[128,1,2,1024]{3,2,1,0:T(2,128)(2,1)S(1)}, u32[]{:S(2)}, u32[]{:S(2)}) %all-to-all-start.1) | async-done | bytes 524320 | tf_op jit(solution)/shard_map/all_to_all | solution.py:176
  137.4 0.9 fusion.6
  138.6 1.2 copy.82
  139.8 4.8 %all-to-all-start.2 = ((bf16[4,128,1,2,256]{4,3,1,2,0:T(2,128)(2,1)}), bf16[4,128,1,2,256]{4,3,1,2,0:T(2,128)(2,1)S(1)}, u32[]{:S(2)}, u32[]{:S(2)}) async-start(bf16[4,128,1,2,256]{4,3,1,2,0:T(2,128)(2,1)} %bitcast.80), calls=%async_computation.2 | async-start | bytes 1048576 | tf_op jit(solution)/shard_map/all_to_all | solution.py:33
  145.0 10.0 %all-to-all-done.2 = bf16[4,128,1,2,256]{4,3,1,2,0:T(2,128)(2,1)S(1)} async-done(((bf16[4,128,1,2,256]{4,3,1,2,0:T(2,128)(2,1)}), bf16[4,128,1,2,256]{4,3,1,2,0:T(2,128)(2,1)S(1)}, u32[]{:S(2)}, u32[]{:S(2)}) %all-to-all-start.2) | async-done | bytes 524320 | tf_op jit(solution)/shard_map/all_to_all | solution.py:33
  155.0 1.3 reduce_sum.121
  156.3 5.8 %all-to-all-start.3 = ((bf16[128,1,2,256]{3,2,1,0:T(2,128)(2,1)}), bf16[128,1,2,256]{3,2,1,0:T(2,128)(2,1)S(1)}, u32[]{:S(2)}, u32[]{:S(2)}) async-start(bf16[128,1,2,256]{3,2,1,0:T(2,128)(2,1)} %bitcast.7), calls=%async_computation.3 | async-start | bytes 262144 | tf_op jit(solution)/shard_map/all_to_all | solution.py:189
  162.4 2.2 copy.81
  165.1 14.3 %all-to-all-done.3 = bf16[128,1,2,256]{3,2,1,0:T(2,128)(2,1)S(1)} async-done(((bf16[128,1,2,256]{3,2,1,0:T(2,128)(2,1)}), bf16[128,1,2,256]{3,2,1,0:T(2,128)(2,1)S(1)}, u32[]{:S(2)}, u32[]{:S(2)}) %all-to-all-start.3) | async-done | bytes 131104 | tf_op jit(solution)/shard_map/all_to_all | solution.py:189
  179.5 70.4 %all-gather.5.cloned.1.call-done = bf16[1024,1024]{1,0:T(8,128)(2,1)} async-done(((bf16[8,1024]{1,0:T(8,128)(2,1)}), bf16[1024,1024]{1,0:T(8,128)(2,1)}) %all-gather.5.cloned.1.call-update) | async-done | bytes 2097168 | tf_op jit(solution)/shard_map/all_gather | solution.py:204
  249.9 2.4 fusion.47
  252.3 0.7 fusion.8
  253.0 0.9 copy.71
  253.9 12.2 %all-to-all-start.4 = ((bf16[128,8,22]{2,1,0:T(8,128)(2,1)}), bf16[128,8,22]{2,1,0:T(8,128)(2,1)S(1)}, u32[]{:S(2)}, u32[]{:S(2)}) async-start(bf16[128,8,22]{2,1,0:T(8,128)(2,1)} %bitcast.9), calls=%async_computation.4 | async-start | bytes 524288 | tf_op jit(solution)/shard_map/all_to_all | solution.py:208
  266.2 22.4 %all-to-all-done.4 = bf16[128,8,22]{2,1,0:T(8,128)(2,1)S(1)} async-done(((bf16[128,8,22]{2,1,0:T(8,128)(2,1)}), bf16[128,8,22]{2,1,0:T(8,128)(2,1)S(1)}, u32[]{:S(2)}, u32[]{:S(2)}) %all-to-all-start.4) | async-done | bytes 45088 | tf_op jit(solution)/shard_map/all_to_all | solution.py:208
  290.1 4.3 %all-to-all-start.5 = ((f32[4,1,16]{2,1,0:T(1,128)}), f32[4,1,16]{2,1,0:T(1,128)S(1)}, u32[]{:S(2)}, u32[]{:S(2)}) async-start(f32[4,1,16]{2,1,0:T(1,128)} %broadcast_in_dim.60), calls=%async_computation.5 | async-start | bytes 4096 | tf_op jit(solution)/shard_map/all_to_all | solution.py:17
  294.4 0.7 pad_maximum_fusion
  295.0 4.6 %all-to-all-done.5 = f32[4,1,16]{2,1,0:T(1,128)S(1)} async-done(((f32[4,1,16]{2,1,0:T(1,128)}), f32[4,1,16]{2,1,0:T(1,128)S(1)}, u32[]{:S(2)}, u32[]{:S(2)}) %all-to-all-start.5) | async-done | bytes 288 | tf_op jit(solution)/shard_map/all_to_all | solution.py:17
  299.7 0.7 multiply_convert_fusion.1
  (99 shorter events, 6.7 us)
Async XLA Ops:
  7.2 26.3 %copy-start = (bf16[128,1024]{1,0:T(8,128)(2,1)S(1)}, bf16[128,1024]{1,0:T(8,128)(2,1)}, u32[]{:S(2)}) copy-start(bf16[128,1024]{1,0:T(8,128)(2,1)} %param.28) | copy-start | bytes 786436
  7.2 25.0 %copy-start.16 = (bf16[8,1,1024,128]{3,2,1,0:T(8,128)(2,1)S(1)}, bf16[8,1,1024,128]{3,2,1,0:T(8,128)(2,1)}, u32[]{:S(2)}) copy-start(bf16[8,1,1024,128]{3,2,1,0:T(8,128)(2,1)} %param.21) | copy-start | bytes 6291460
  32.0 1.6 copy-start.15
  32.2 6.6 %copy-start.10 = (bf16[22,256]{1,0:T(8,128)(2,1)S(1)}, bf16[22,256]{1,0:T(8,128)(2,1)}, u32[]{:S(2)}) copy-start(bf16[22,256]{1,0:T(8,128)(2,1)} %param.37) | copy-start | bytes 33796
  33.3 54.4 %copy-start.12 = (s32[8,2]{0,1:T(2,128)S(1)}, s32[8,2]{0,1:T(2,128)}, u32[]{:S(2)}) copy-start(s32[8,2]{0,1:T(2,128)} %param.31) | copy-start | bytes 196
  33.3 55.0 %copy-start.2 = (bf16[8,1024]{1,0:T(8,128)(2,1)S(1)}, bf16[8,1024]{1,0:T(8,128)(2,1)}, u32[]{:S(2)}) copy-start(bf16[8,1024]{1,0:T(8,128)(2,1)} %param.20) | copy-start | bytes 49156
  33.3 55.3 %copy-start.11 = (f32[1024]{0:T(1024)S(1)}, f32[1024]{0:T(1024)}, u32[]{:S(2)}) copy-start(f32[1024]{0:T(1024)} %param.29) | copy-start | bytes 12292
  34.3 54.0 %all-to-all-start = ((bf16[4,8,1024]{2,1,0:T(8,128)(2,1)}), bf16[4,8,1024]{2,1,0:T(8,128)(2,1)S(1)}, u32[]{:S(2)}, u32[]{:S(2)}) async-start(bf16[4,8,1024]{2,1,0:T(8,128)(2,1)} %broadcast_in_dim.35), calls=%async_computation | async-start | bytes 131072 | tf_op jit(solution)/shard_map/all_to_all | solution.py:17
  38.8 123.7 %all-gather.7.cloned.1.call-start = ((), (), s32[]{:S(2)}) async-start(), calls=%async_computation.7 | async-start | bytes 2162688 | tf_op jit(solution)/shard_map/all_gather | solution.py:46
  73.2 30.5 %copy-start.5 = (bf16[1024,64]{0,1:T(8,128)(2,1)S(1)}, bf16[1024,64]{0,1:T(8,128)(2,1)}, u32[]{:S(2)}) copy-start(bf16[1024,64]{0,1:T(8,128)(2,1)} %param.24) | copy-start | bytes 393220
  73.2 30.7 %copy-start.6 = (bf16[1024,64]{0,1:T(8,128)(2,1)S(1)}, bf16[1024,64]{0,1:T(8,128)(2,1)}, u32[]{:S(2)}) copy-start(bf16[1024,64]{0,1:T(8,128)(2,1)} %param.25) | copy-start | bytes 393220
  87.7 49.4 %copy-start.4 = (bf16[1024,112]{0,1:T(8,128)(2,1)S(1)}, bf16[1024,112]{0,1:T(8,128)(2,1)}, u32[]{:S(2)}) copy-start(bf16[1024,112]{0,1:T(8,128)(2,1)} %param.32) | copy-start | bytes 688132
  87.7 162.3 %all-gather.5.cloned.1.call-start = ((), (), s32[]{:S(2)}) async-start(), calls=%async_computation.6 | async-start | bytes 2113536 | tf_op jit(solution)/shard_map/all_gather | solution.py:204
  89.6 47.8 %copy-start.17 = (bf16[112,1024]{1,0:T(8,128)(2,1)S(1)}, bf16[112,1024]{1,0:T(8,128)(2,1)}, u32[]{:S(2)}) copy-start(bf16[112,1024]{1,0:T(8,128)(2,1)} %param.34) | copy-start | bytes 688132
  89.6 47.8 %copy-start.18 = (bf16[1024,112]{0,1:T(8,128)(2,1)S(1)}, bf16[1024,112]{0,1:T(8,128)(2,1)}, u32[]{:S(2)}) copy-start(bf16[1024,112]{0,1:T(8,128)(2,1)} %param.33) | copy-start | bytes 688132
  91.7 45.1 %all-to-all-start.1 = ((bf16[128,1,2,1024]{3,2,1,0:T(2,128)(2,1)}), bf16[128,1,2,1024]{3,2,1,0:T(2,128)(2,1)S(1)}, u32[]{:S(2)}, u32[]{:S(2)}) async-start(bf16[128,1,2,1024]{3,2,1,0:T(2,128)(2,1)} %bitcast.5), calls=%async_computation.1 | async-start | bytes 1048576 | tf_op jit(solution)/shard_map/all_to_all | solution.py:176
  137.4 7.3 %copy-start.13 = (bf16[1024]{0:T(1024)(128)(2,1)S(1)}, bf16[1024]{0:T(1024)(128)(2,1)}, u32[]{:S(2)}) copy-start(bf16[1024]{0:T(1024)(128)(2,1)} %param.38) | copy-start | bytes 6148
  137.4 7.3 %copy-start.3 = (bf16[8,1024]{1,0:T(8,128)(2,1)S(1)}, bf16[8,1024]{1,0:T(8,128)(2,1)}, u32[]{:S(2)}) copy-start(bf16[8,1024]{1,0:T(8,128)(2,1)} %multiply_convert_fusion) | copy-start | bytes 49156
  137.4 7.3 %copy-start.9 = (bf16[1024,16]{0,1:T(8,128)(2,1)S(1)}, bf16[1024,16]{0,1:T(8,128)(2,1)}, u32[]{:S(2)}) copy-start(bf16[1024,16]{0,1:T(8,128)(2,1)} %param.30) | copy-start | bytes 98308
  139.8 15.1 %all-to-all-start.2 = ((bf16[4,128,1,2,256]{4,3,1,2,0:T(2,128)(2,1)}), bf16[4,128,1,2,256]{4,3,1,2,0:T(2,128)(2,1)S(1)}, u32[]{:S(2)}, u32[]{:S(2)}) async-start(bf16[4,128,1,2,256]{4,3,1,2,0:T(2,128)(2,1)} %bitcast.80), calls=%async_computation.2 | async-start | bytes 1048576 | tf_op jit(solution)/shard_map/all_to_all | solution.py:33
  156.3 23.0 %all-to-all-start.3 = ((bf16[128,1,2,256]{3,2,1,0:T(2,128)(2,1)}), bf16[128,1,2,256]{3,2,1,0:T(2,128)(2,1)S(1)}, u32[]{:S(2)}, u32[]{:S(2)}) async-start(bf16[128,1,2,256]{3,2,1,0:T(2,128)(2,1)} %bitcast.7), calls=%async_computation.3 | async-start | bytes 262144 | tf_op jit(solution)/shard_map/all_to_all | solution.py:189
  164.6 85.3 %copy-start.7 = (bf16[1024,22]{0,1:T(8,128)(2,1)S(1)}, bf16[1024,22]{0,1:T(8,128)(2,1)}, u32[]{:S(2)}) copy-start(bf16[1024,22]{0,1:T(8,128)(2,1)} %param.35) | copy-start | bytes 135172
  165.1 87.2 %copy-start.8 = (bf16[1024,22]{0,1:T(8,128)(2,1)S(1)}, bf16[1024,22]{0,1:T(8,128)(2,1)}, u32[]{:S(2)}) copy-start(bf16[1024,22]{0,1:T(8,128)(2,1)} %param.36) | copy-start | bytes 135172
  249.9 2.4 copy-start.1
  253.0 46.7 %copy-start.14 = (f32[256]{0:T(256)S(1)}, f32[256]{0:T(256)}, u32[]{:S(2)}) copy-start(f32[256]{0:T(256)} %param.39) | copy-start | bytes 3076
  253.9 34.7 %all-to-all-start.4 = ((bf16[128,8,22]{2,1,0:T(8,128)(2,1)}), bf16[128,8,22]{2,1,0:T(8,128)(2,1)S(1)}, u32[]{:S(2)}, u32[]{:S(2)}) async-start(bf16[128,8,22]{2,1,0:T(8,128)(2,1)} %bitcast.9), calls=%async_computation.4 | async-start | bytes 524288 | tf_op jit(solution)/shard_map/all_to_all | solution.py:208
  290.1 9.5 %all-to-all-start.5 = ((f32[4,1,16]{2,1,0:T(1,128)}), f32[4,1,16]{2,1,0:T(1,128)S(1)}, u32[]{:S(2)}, u32[]{:S(2)}) async-start(f32[4,1,16]{2,1,0:T(1,128)} %broadcast_in_dim.60), calls=%async_computation.5 | async-start | bytes 4096 | tf_op jit(solution)/shard_map/all_to_all | solution.py:17
Sparse Core Ops, SparseCore 0:
  87.8 17.4 all-gather.6
  108.4 141.4 all-gather.4
where the time goes:
time: 308 us; the launch traced here: 307 us
  waiting for transfers between devices  154 us (50%)
  blocking collectives  48.8 us (16%)
  starting transfers between devices  43.6 us (14%)
  other arithmetic  25.7 us (8%)
  between operations  14.5 us (5%)
  matrix products  11.1 us (4%)
  local copies, waits for them, and re-layouts  9.16 us (3%)
    all_gather x1, waiting for transfers between devices, body(): shard_rows = lax.all_gather(settled, EP, axis=0, tiled=True)  70.4 us
    all_gather x2, blocking collectives, stacked_from(): tiles = lax.all_gather(tiles, axes[k], axis=0, tiled=True)  48.8 us
    all_to_all x1, waiting for transfers between devices, body(): lax.all_to_all(outgoing, EP, split_axis=0, concat_axis=0, tiled=True)  32.8 us
    all_to_all x1, waiting for transfers between devices, body(): lax.all_to_all(dense_hidden, EP, split_axis=0, concat_axis=1, tiled=True)  22.4 us
    another operation x2, other arithmetic  20.1 us
    all_to_all x1, waiting for transfers between devices, body(): lax.all_to_all(summed.astype(jnp.bfloat16), EP, split_axis=0, concat_axis...  14.3 us
    all_to_all x1, starting transfers between devices, body(): lax.all_to_all(dense_hidden, EP, split_axis=0, concat_axis=1, tiled=True)  12.2 us
    all_to_all x1, starting transfers between devices, body(): lax.all_to_all(outgoing, EP, split_axis=0, concat_axis=0, tiled=True)  12 us
  transfers between devices with their start and end apart: 8, of which 6 were waited for; matrix products, arithmetic and copies ran while one was open for 4% of the time, Pallas kernels for 0%

commit v1 on v0

--- a/solution.py
+++ b/solution.py
@@ -201,7 +201,10 @@
     routed = jnp.dot(weighted, gathered, precision=PRECISE)
     column_rank = lax.axis_index("tp")
     own_settled = lax.dynamic_slice_in_dim(settled, column_rank * slice_width, slice_width, 1)
-    shard_rows = lax.all_gather(settled, EP, axis=0, tiled=True)
+    devices = lax.axis_size(EP)
+    blocks = jnp.stack([settled for _ in range(devices)])
+    blocks = lax.all_to_all(blocks, EP, split_axis=0, concat_axis=0)
+    shard_rows = jnp.concatenate(blocks, axis=0)
     gate_pre = jnp.dot(shard_rows, dense_gate, preferred_element_type=jnp.float32)
     up_pre = jnp.dot(shard_rows, dense_up, preferred_element_type=jnp.float32)
     dense_hidden = (jax.nn.silu(gate_pre) * up_pre).astype(jnp.bfloat16)

time: 308 us -> 363 us (1.18)
  blocking collectives: 48.8 us -> 165 us
  waiting for transfers between devices: 154 us -> 82.2 us
  starting transfers between devices: 43.6 us -> 50.4 us
  local copies, waits for them, and re-layouts: 9.16 us -> 14 us
    all_gather x2, blocking collectives: 48.8 us -> 130 us  [stacked_from(): tiles = lax.all_gather(tiles, axes[k], axis=0, tiled=True)]
    all_gather x1 -> x0, waiting for transfers between devices: 70.4 us -> none  [body(): shard_rows = lax.all_gather(settled, EP, axis=0, tiled=True)]
    all_to_all x0 -> x2, blocking collectives: none -> 35.8 us  [the longest x1 22.8 us: body(): lax.all_to_all(summed.astype(jnp.bfloat16), EP, split_axis=0, concat_axis...]
    all_to_all x2 -> x1, waiting for transfers between devices: 24.2 us -> 0.01 us  [body(): blocks = lax.all_to_all(blocks, EP, split_axis=0, concat_axis=0)]
    all_gather x1, waiting for transfers between devices: 0.01 us -> 17.3 us  [stacked_from(): tiles = lax.all_gather(tiles, axes[k], axis=0, tiled=True)]
    all_to_all x1, starting transfers between devices: 12 us -> 19 us  [body(): lax.all_to_all(outgoing, EP, split_axis=0, concat_axis=0, tiled=True)]
    all_to_all x2, waiting for transfers between devices: 4.56 us -> 9.37 us  [from_everyone(): return lax.all_to_all(copies, axis, split_axis=0, concat_axis=0, tiled=True)]
    all_to_all x2 -> x1, starting transfers between devices: 10.6 us -> 6.2 us  [body(): blocks = lax.all_to_all(blocks, EP, split_axis=0, concat_axis=0)]
  transfers between devices with their start and end apart: 8 -> 6, of which waited for: 6 -> 5; matrix products, arithmetic and copies ran while one was open for 4% -> 3% of each run, Pallas kernels for 0% -> 0%
where the time goes in v1:
time: 363 us; the launch traced here: 362 us
  blocking collectives  165 us (45%)
  waiting for transfers between devices  82.2 us (23%)
  starting transfers between devices  50.4 us (14%)
  other arithmetic  24.4 us (7%)
  between operations  14.4 us (4%)
  local copies, waits for them, and re-layouts  14 us (4%)
  matrix products  11.6 us (3%)
    all_gather x2, blocking collectives, stacked_from(): tiles = lax.all_gather(tiles, axes[k], axis=0, tiled=True)  130 us
    all_to_all x1, waiting for transfers between devices, body(): lax.all_to_all(outgoing, EP, split_axis=0, concat_axis=0, tiled=True)  33.1 us
    all_to_all x1, blocking collectives, body(): lax.all_to_all(summed.astype(jnp.bfloat16), EP, split_axis=0, concat_axis...  22.8 us
    all_to_all x1, waiting for transfers between devices, body(): lax.all_to_all(dense_hidden, EP, split_axis=0, concat_axis=1, tiled=True)  22.4 us
    another operation x2, other arithmetic  20.1 us
    all_to_all x1, starting transfers between devices, body(): lax.all_to_all(outgoing, EP, split_axis=0, concat_axis=0, tiled=True)  19 us
    all_gather x1, waiting for transfers between devices, stacked_from(): tiles = lax.all_gather(tiles, axes[k], axis=0, tiled=True)  17.3 us
    all_to_all x1, starting transfers between devices, body(): lax.all_to_all(dense_hidden, EP, split_axis=0, concat_axis=1, tiled=True)  16.4 us
  transfers between devices with their start and end apart: 6, of which 5 were waited for; matrix products, arithmetic and copies ran while one was open for 3% of the time, Pallas kernels for 0%

profile of v1, /device:TPU:32, one launch (start us, length us, event | category | flops | bytes accessed | tf_op | source)
XLA Modules:
  0.0 362.5 jit_solution(17378950936821138203)
XLA Ops:
  7.2 0.8 iota_compare_fusion
  8.0 1.1 convolution_convert_fusion.4
  9.1 2.3 fusion.40
  11.5 19.8 %reduce-window.6 = f32[8,1,2,8,128]{4,3,2,1,0:T(8,128)S(1)} reduce-window(f32[8,1,2,8,128]{4,3,2,1,0:T(8,128)S(1)} %bitcast.97, f32[]{:T(128)} %constant.108.clone.1), window={size=1x1x1x1x128 pad=0_0x0_0x0_0x0_0x0_127}, to_apply=%region_0.1 | reduce-window | flops 2080768 | bytes 131076 | tf_op jit(solution)/shard_map/reduce-window
  32.1 2.7 multiply_reduce_fusion.3
  35.2 0.6 broadcast_in_dim.35
  35.8 4.5 %all-to-all-start = ((bf16[4,8,1024]{2,1,0:T(8,128)(2,1)}), bf16[4,8,1024]{2,1,0:T(8,128)(2,1)S(1)}, u32[]{:S(2)}, u32[]{:S(2)}) async-start(bf16[4,8,1024]{2,1,0:T(8,128)(2,1)} %broadcast_in_dim.35), calls=%async_computation | async-start | bytes 131072 | tf_op jit(solution)/shard_map/all_to_all | solution.py:17
  41.1 4.8 %all-to-all-done = bf16[4,8,1024]{2,1,0:T(8,128)(2,1)S(1)} async-done(((bf16[4,8,1024]{2,1,0:T(8,128)(2,1)}), bf16[4,8,1024]{2,1,0:T(8,128)(2,1)S(1)}, u32[]{:S(2)}, u32[]{:S(2)}) %all-to-all-start) | async-done | bytes 65568 | tf_op jit(solution)/shard_map/all_to_all | solution.py:17
  46.6 1.1 broadcast_in_dim.58
  47.6 19.0 %all-to-all-start.1 = ((bf16[128,1,2,1024]{3,2,1,0:T(2,128)(2,1)}), bf16[128,1,2,1024]{3,2,1,0:T(2,128)(2,1)S(1)}, u32[]{:S(2)}, u32[]{:S(2)}) async-start(bf16[128,1,2,1024]{3,2,1,0:T(2,128)(2,1)} %bitcast.5), calls=%async_computation.1 | async-start | bytes 1048576 | tf_op jit(solution)/shard_map/all_to_all | solution.py:176
  66.7 33.1 %all-to-all-done.1 = bf16[128,1,2,1024]{3,2,1,0:T(2,128)(2,1)S(1)} async-done(((bf16[128,1,2,1024]{3,2,1,0:T(2,128)(2,1)}), bf16[128,1,2,1024]{3,2,1,0:T(2,128)(2,1)S(1)}, u32[]{:S(2)}, u32[]{:S(2)}) %all-to-all-start.1) | async-done | bytes 524320 | tf_op jit(solution)/shard_map/all_to_all | solution.py:176
  100.3 0.9 fusion.10
  102.0 13.0 %all_to_all.50 = bf16[4,128,1,2,256]{4,3,1,2,0:T(2,128)(2,1)S(1)} all-to-all(bf16[4,128,1,2,256]{4,3,1,2,0:T(2,128)(2,1)S(1)} %bitcast.90), channel_id=1, replica_groups=mesh['ep_0'=16,'ep_1'=4,'ep_2'=2,'tp'=4] {'tp'}, dimensions={0} | all-to-all | bytes 1048576 | tf_op jit(solution)/shard_map/all_to_all | solution.py:33
  115.0 0.7 reduce_sum.121
  115.7 22.8 %all_to_all.51 = bf16[128,1,2,256]{3,2,1,0:T(2,128)(2,1)S(1)} all-to-all(bf16[128,1,2,256]{3,2,1,0:T(2,128)(2,1)S(1)} %bitcast.96), channel_id=1, replica_groups=mesh['ep_0'=16,'ep_1'=4,'ep_2'=2,'tp'=4] {'ep_0','ep_1','ep_2'}, dimensions={0} | all-to-all | bytes 262144 | tf_op jit(solution)/shard_map/all_to_all | solution.py:189
  138.4 1.6 stack.2
  140.1 6.2 %all-to-all-start.4 = ((bf16[128,8,1024]{2,1,0:T(8,128)(2,1)}), bf16[128,8,1024]{2,1,0:T(8,128)(2,1)S(1)}, u32[]{:S(2)}, u32[]{:S(2)}) async-start(bf16[128,8,1024]{2,1,0:T(8,128)(2,1)} %stack.2), calls=%async_computation.4 | async-start | bytes 4194304 | tf_op jit(solution)/shard_map/all_to_all | solution.py:206
  146.4 115.0 %all-gather.1 = bf16[16,22,256]{2,1,0:T(8,128)(2,1)S(1)} all-gather(bf16[1,22,256]{2,1,0:T(8,128)(2,1)S(1)} %bitcast.99), channel_id=2, replica_groups=mesh['ep_0'=16,'ep_1'=4,'ep_2'=2,'tp'=4] {'ep_0'}, dimensions={0}, use_global_device_ids=true | all-gather | bytes 191488 | tf_op jit(solution)/shard_map/all_gather | solution.py:46
  261.4 14.7 %all_gather.10 = bf16[64,22,256]{2,0,1:T(8,128)(2,1)} all-gather(bf16[16,22,256]{2,0,1:T(8,128)(2,1)S(1)} %copy.73), channel_id=1, replica_groups=mesh['ep_0'=16,'ep_1'=4,'ep_2'=2,'tp'=4] {'ep_1'}, dimensions={0}, use_global_device_ids=true | all-gather | bytes 901120 | tf_op jit(solution)/shard_map/all_gather | solution.py:46
  277.1 17.3 %all-gather.4.cloned.1.call-done = bf16[128,22,256]{2,0,1:T(8,128)(2,1)} async-done(((bf16[64,22,256]{2,0,1:T(8,128)(2,1)}), bf16[128,22,256]{2,0,1:T(8,128)(2,1)}) %all-gather.4.cloned.1.call-update) | async-done | bytes 1441808 | tf_op jit(solution)/shard_map/all_gather | solution.py:46
  294.5 3.3 copy.81
  297.8 3.4 reshape_reshape.7
  301.4 0.7 fusion.6
  302.0 0.7 fusion.15
  302.7 0.9 copy.71
  303.6 16.4 %all-to-all-start.5 = ((bf16[128,8,22]{2,1,0:T(8,128)(2,1)}), bf16[128,8,22]{2,1,0:T(8,128)(2,1)S(1)}, u32[]{:S(2)}, u32[]{:S(2)}) async-start(bf16[128,8,22]{2,1,0:T(8,128)(2,1)} %bitcast.10), calls=%async_computation.5 | async-start | bytes 524288 | tf_op jit(solution)/shard_map/all_to_all | solution.py:211
  320.1 22.4 %all-to-all-done.5 = bf16[128,8,22]{2,1,0:T(8,128)(2,1)S(1)} async-done(((bf16[128,8,22]{2,1,0:T(8,128)(2,1)}), bf16[128,8,22]{2,1,0:T(8,128)(2,1)S(1)}, u32[]{:S(2)}, u32[]{:S(2)}) %all-to-all-start.5) | async-done | bytes 45088 | tf_op jit(solution)/shard_map/all_to_all | solution.py:211
  342.9 1.8 fusion.53
  345.4 4.3 %all-to-all-start.6 = ((f32[4,1,16]{2,1,0:T(1,128)}), f32[4,1,16]{2,1,0:T(1,128)S(1)}, u32[]{:S(2)}, u32[]{:S(2)}) async-start(f32[4,1,16]{2,1,0:T(1,128)} %broadcast_in_dim.60), calls=%async_computation.6 | async-start | bytes 4096 | tf_op jit(solution)/shard_map/all_to_all | solution.py:17
  349.6 0.7 pad_maximum_fusion
  350.3 4.6 %all-to-all-done.6 = f32[4,1,16]{2,1,0:T(1,128)S(1)} async-done(((f32[4,1,16]{2,1,0:T(1,128)}), f32[4,1,16]{2,1,0:T(1,128)S(1)}, u32[]{:S(2)}, u32[]{:S(2)}) %all-to-all-start.6) | async-done | bytes 288 | tf_op jit(solution)/shard_map/all_to_all | solution.py:17
  354.9 0.7 multiply_convert_fusion.1
  (91 shorter events, 6.5 us)
Async XLA Ops:
  7.2 27.8 %copy-start = (bf16[128,1024]{1,0:T(8,128)(2,1)S(1)}, bf16[128,1024]{1,0:T(8,128)(2,1)}, u32[]{:S(2)}) copy-start(bf16[128,1024]{1,0:T(8,128)(2,1)} %param.28) | copy-start | bytes 786436
  31.8 3.2 copy-start.13
  32.1 8.2 %copy-start.10 = (s32[8,2]{0,1:T(2,128)S(1)}, s32[8,2]{0,1:T(2,128)}, u32[]{:S(2)}) copy-start(s32[8,2]{0,1:T(2,128)} %param.31) | copy-start | bytes 196
  32.1 13.8 %copy-start.1 = (bf16[8,1024]{1,0:T(8,128)(2,1)S(1)}, bf16[8,1024]{1,0:T(8,128)(2,1)}, u32[]{:S(2)}) copy-start(bf16[8,1024]{1,0:T(8,128)(2,1)} %param.20) | copy-start | bytes 49156
  32.1 14.2 %copy-start.9 = (f32[1024]{0:T(1024)S(1)}, f32[1024]{0:T(1024)}, u32[]{:S(2)}) copy-start(f32[1024]{0:T(1024)} %param.29) | copy-start | bytes 12292
  34.8 65.2 %copy-start.2 = (bf16[1024,112]{0,1:T(8,128)(2,1)S(1)}, bf16[1024,112]{0,1:T(8,128)(2,1)}, u32[]{:S(2)}) copy-start(bf16[1024,112]{0,1:T(8,128)(2,1)} %param.32) | copy-start | bytes 688132
  35.8 10.1 %all-to-all-start = ((bf16[4,8,1024]{2,1,0:T(8,128)(2,1)}), bf16[4,8,1024]{2,1,0:T(8,128)(2,1)S(1)}, u32[]{:S(2)}, u32[]{:S(2)}) async-start(bf16[4,8,1024]{2,1,0:T(8,128)(2,1)} %broadcast_in_dim.35), calls=%async_computation | async-start | bytes 131072 | tf_op jit(solution)/shard_map/all_to_all | solution.py:17
  41.0 59.3 %copy-start.14 = (bf16[112,1024]{1,0:T(8,128)(2,1)S(1)}, bf16[112,1024]{1,0:T(8,128)(2,1)}, u32[]{:S(2)}) copy-start(bf16[112,1024]{1,0:T(8,128)(2,1)} %param.34) | copy-start | bytes 688132
  41.0 59.3 %copy-start.15 = (bf16[1024,112]{0,1:T(8,128)(2,1)S(1)}, bf16[1024,112]{0,1:T(8,128)(2,1)}, u32[]{:S(2)}) copy-start(bf16[1024,112]{0,1:T(8,128)(2,1)} %param.33) | copy-start | bytes 688132
  47.6 52.2 %all-to-all-start.1 = ((bf16[128,1,2,1024]{3,2,1,0:T(2,128)(2,1)}), bf16[128,1,2,1024]{3,2,1,0:T(2,128)(2,1)S(1)}, u32[]{:S(2)}, u32[]{:S(2)}) async-start(bf16[128,1,2,1024]{3,2,1,0:T(2,128)(2,1)} %bitcast.5), calls=%async_computation.1 | async-start | bytes 1048576 | tf_op jit(solution)/shard_map/all_to_all | solution.py:176
  140.1 6.3 %copy-start.8 = (bf16[22,256]{1,0:T(8,128)(2,1)S(1)}, bf16[22,256]{1,0:T(8,128)(2,1)}, u32[]{:S(2)}) copy-start(bf16[22,256]{1,0:T(8,128)(2,1)} %param.37) | copy-start | bytes 33796
  140.1 161.3 %all-to-all-start.4 = ((bf16[128,8,1024]{2,1,0:T(8,128)(2,1)}), bf16[128,8,1024]{2,1,0:T(8,128)(2,1)S(1)}, u32[]{:S(2)}, u32[]{:S(2)}) async-start(bf16[128,8,1024]{2,1,0:T(8,128)(2,1)} %stack.2), calls=%async_computation.4 | async-start | bytes 4194304 | tf_op jit(solution)/shard_map/all_to_all | solution.py:206
  146.3 129.9 %copy-start.11 = (bf16[1024]{0:T(1024)(128)(2,1)S(1)}, bf16[1024]{0:T(1024)(128)(2,1)}, u32[]{:S(2)}) copy-start(bf16[1024]{0:T(1024)(128)(2,1)} %param.38) | copy-start | bytes 6148
  146.3 129.9 %copy-start.3 = (bf16[1024,64]{0,1:T(8,128)(2,1)S(1)}, bf16[1024,64]{0,1:T(8,128)(2,1)}, u32[]{:S(2)}) copy-start(bf16[1024,64]{0,1:T(8,128)(2,1)} %param.24) | copy-start | bytes 393220
  146.3 130.0 %copy-start.4 = (bf16[1024,64]{0,1:T(8,128)(2,1)S(1)}, bf16[1024,64]{0,1:T(8,128)(2,1)}, u32[]{:S(2)}) copy-start(bf16[1024,64]{0,1:T(8,128)(2,1)} %param.25) | copy-start | bytes 393220
  146.3 130.2 %copy-start.7 = (bf16[1024,16]{0,1:T(8,128)(2,1)S(1)}, bf16[1024,16]{0,1:T(8,128)(2,1)}, u32[]{:S(2)}) copy-start(bf16[1024,16]{0,1:T(8,128)(2,1)} %param.30) | copy-start | bytes 98308
  146.3 148.1 %all-gather.4.cloned.1.call-start = ((), (), s32[]{:S(2)}) async-start(), calls=%async_computation.7 | async-start | bytes 2162688 | tf_op jit(solution)/shard_map/all_gather | solution.py:46
  297.8 3.6 copy-start.5
  301.2 0.8 copy-start.6
  302.7 52.3 %copy-start.12 = (f32[256]{0:T(256)S(1)}, f32[256]{0:T(256)}, u32[]{:S(2)}) copy-start(f32[256]{0:T(256)} %param.39) | copy-start | bytes 3076
  303.6 38.9 %all-to-all-start.5 = ((bf16[128,8,22]{2,1,0:T(8,128)(2,1)}), bf16[128,8,22]{2,1,0:T(8,128)(2,1)S(1)}, u32[]{:S(2)}, u32[]{:S(2)}) async-start(bf16[128,8,22]{2,1,0:T(8,128)(2,1)} %bitcast.10), calls=%async_computation.5 | async-start | bytes 524288 | tf_op jit(solution)/shard_map/all_to_all | solution.py:211
  345.4 9.5 %all-to-all-start.6 = ((f32[4,1,16]{2,1,0:T(1,128)}), f32[4,1,16]{2,1,0:T(1,128)S(1)}, u32[]{:S(2)}, u32[]{:S(2)}) async-start(f32[4,1,16]{2,1,0:T(1,128)} %broadcast_in_dim.60), calls=%async_computation.6 | async-start | bytes 4096 | tf_op jit(solution)/shard_map/all_to_all | solution.py:17
Sparse Core Ops, SparseCore 0:
  276.2 18.1 all-gather.3
